TPU v7x, 32 devices: a whole 2x2x4 slice. The times are simulated.
32 devices in a mesh: ep: 8 (over z, y), tp: 4 (over x, core).
Axes of the slice: x: 2, y: 2, z: 4, core: 2. Of those that a mesh axis runs over, the one named last changes fastest.
Arguments:
- tokens: bfloat16 [6144, 2048], P('ep', 'tp')
- norm_gain: float32 [2048], P('tp'), may hold values from 0.1 to 1.9
- routing: int32 [6144, 2], P('ep'), may hold values from 0 to 7, as said below
- route_weight: float32 [6144, 2], P('ep'), may hold values from 0.2 to 1
- w_gate: bfloat16 [8, 2048, 512], P('ep', 'tp'), may hold values from -0.125 to 0.125
- w_up: bfloat16 [8, 2048, 512], P('ep', 'tp'), may hold values from -0.125 to 0.125
- w_down: bfloat16 [8, 512, 2048], P('ep', None, 'tp'), may hold values from -0.25 to 0.25
- w_branch_in: bfloat16 [2048, 1024], P('ep', 'tp'), may hold values from -0.125 to 0.125
- w_branch_out: bfloat16 [1024, 2048], P('tp', 'ep'), may hold values from -0.1875 to 0.1875
- branch_gate: float32 [2048], P('tp'), may hold values from -3 to 3
Outputs:
- mixed: bfloat16 [6144, 2048], P('ep', 'tp')
Inputs may be any that keep to these rules, and one draw needn't show every extreme that they name: `routing`: each row names two different experts of the same group; expert e belongs to group e // 2. Among the rows of one device (aligned blocks of 768 rows) no expert is named more than 384 times, and in every block all experts of one group are named exactly 384 times.
All inputs are finite; a program needn't handle non-finite values.
Results may differ from a plain program's by a relative error of at most 0.0069.
Values may be sent and summed in bfloat16 or wider, within the bound.
A program may use at most 128 MiB of HBM per device.

v0:
```python
import jax
import jax.numpy as jnp
from jax import lax
from jax.sharding import PartitionSpec as P

GROUPS = 4


epsilon = 1e-06


def send_back(result):
    return lax.all_to_all(result, "ep", split_axis=0, concat_axis=0, tiled=True)


def body(
    tokens,
    norm_gain,
    routing,
    route_weight,
    w_gate,
    w_up,
    w_down,
    w_branch_in,
    w_branch_out,
    branch_gate,
):
    token_count, quarter = tokens.shape
    full_width = quarter * lax.axis_size("tp")
    floats = tokens.astype(jnp.float32)
    squares = lax.psum(jnp.sum(floats * floats, axis=1), "tp")
    normed = (floats * lax.rsqrt(squares[:, None] / full_width + epsilon) * norm_gain).astype(
        jnp.bfloat16
    )
    expert_count = lax.axis_size("ep") * w_gate.shape[0]
    capacity = token_count // (expert_count // GROUPS)
    flat_ids = routing.reshape(-1)
    one_hot = (flat_ids[:, None] == jnp.arange(expert_count, dtype=jnp.int32)[None, :]).astype(
        jnp.int32
    )
    before = jnp.cumsum(one_hot, axis=0) - one_hot
    position = flat_ids * capacity + jnp.sum(before * one_hot, axis=1)
    copies = jnp.repeat(normed, 2, axis=0)
    buffer = jnp.zeros((expert_count * capacity, quarter), jnp.bfloat16).at[position].set(copies)
    buffer = buffer.reshape(expert_count, capacity, quarter)
    gate_whole, up_whole, down_whole = (
        lax.all_gather(w_gate[0], "tp", axis=0, tiled=True),
        lax.all_gather(w_up[0], "tp", axis=0, tiled=True),
        lax.all_gather(w_down[0], "tp", axis=1, tiled=True),
    )
    row_split = lax.all_to_all(
        lax.all_to_all(buffer, "ep", split_axis=0, concat_axis=0, tiled=True),
        "tp",
        split_axis=0,
        concat_axis=2,
        tiled=True,
    )
    slot_rows = row_split.reshape(-1, row_split.shape[2])
    gate_sum = jnp.dot(slot_rows, gate_whole, preferred_element_type=jnp.float32)
    up_sum = jnp.dot(slot_rows, up_whole, preferred_element_type=jnp.float32)
    hidden = (jax.nn.silu(gate_sum) * up_sum).astype(jnp.bfloat16)
    result = jnp.dot(hidden, down_whole, preferred_element_type=jnp.float32).astype(jnp.bfloat16)
    feature_split = lax.all_to_all(
        result.reshape(row_split.shape), "tp", split_axis=2, concat_axis=0, tiled=True
    )
    returned = send_back(feature_split)
    picked = returned.reshape(expert_count * capacity, quarter)[position].reshape(
        token_count, 2, quarter
    )
    routed = jnp.sum(picked.astype(jnp.float32) * route_weight[:, :, None], axis=1)
    branch_tokens = lax.all_to_all(normed, "tp", split_axis=0, concat_axis=1, tiled=True)
    in_cols, out_rows = (
        lax.all_gather(w_branch_in, "tp", axis=1, tiled=True),
        lax.all_gather(w_branch_out, "tp", axis=0, tiled=True),
    )
    in_whole, out_whole = (
        lax.all_gather(in_cols, "ep", axis=0, tiled=True),
        lax.all_gather(out_rows, "ep", axis=1, tiled=True),
    )
    branch_hidden = jax.nn.silu(
        jnp.dot(branch_tokens, in_whole, preferred_element_type=jnp.float32)
    ).astype(jnp.bfloat16)
    branch_local = jnp.dot(branch_hidden, out_whole, preferred_element_type=jnp.float32).astype(
        jnp.bfloat16
    )
    branch = lax.all_to_all(branch_local, "tp", split_axis=1, concat_axis=0, tiled=True)
    return (routed + jax.nn.sigmoid(branch_gate) * branch.astype(jnp.float32)).astype(jnp.bfloat16)


def solution(mesh):
    return jax.shard_map(
        body,
        mesh=mesh,
        in_specs=(
            P("ep", "tp"),
            P("tp"),
            P("ep", None),
            P("ep", None),
            P("ep", "tp", None),
            P("ep", "tp", None),
            P("ep", None, "tp"),
            P("ep", "tp"),
            P("tp", "ep"),
            P("tp"),
        ),
        out_specs=P("ep", "tp"),
        check_vma=False,
    )
```

profile of v0, /device:TPU:0, one launch (start us, length us, event | category | flops | bytes accessed | tf_op | source)
XLA Modules:
  0.0 403.0 jit_solution(17927686198045265100)
XLA Ops:
  6.5 0.0 all-gather.13.cloned.1.call-start
  6.5 0.7 all-gather.13.cloned.1.call-update
  7.3 0.0 copy-start.6
  7.3 0.0 all-gather.15.cloned.1.call-start
  7.3 0.7 all-gather.15.cloned.1.call-update
  8.0 0.0 all-gather.17.cloned.1.call-start
  8.1 0.7 all-gather.17.cloned.1.call-update
  8.8 0.9 copy.30
  9.6 0.7 broadcast_multiply_fusion
  10.3 0.2 eq.29
  10.6 0.0 copy-done.1
  10.6 0.2 fusion.5
  10.8 8.4 %psum.7 = f32[768]{0:T(1024)S(1)} all-reduce(f32[768]{0:T(1024)S(1)} %fusion.5), channel_id=1, replica_groups=mesh['ep'=8,'tp'=4] {'tp'}, use_global_device_ids=true, to_apply=%region_4.5 | all-reduce | flops 768 | bytes 6144 | tf_op jit(solution)/shard_map/psum | solution.py:31
  19.2 2.3 reduce-window.6
  21.5 0.3 slice_reduce_fusion
  21.7 0.2 eq.25
  22.0 0.2 reduce-window.9
  22.1 0.2 copy.29
  22.3 0.3 mul.67
  22.6 0.0 copy-done.6
  22.6 0.2 fusion.7
  22.9 0.0 copy-start
  22.9 0.9 copy-done
  23.7 0.8 broadcast_in_dim.5
  24.5 0.6 reshape.100
  25.2 0.1 add_bitcast_fusion
  25.4 9.5 %scatter_custom_fusion = bf16[3072,512]{1,0:T(8,128)(2,1)} fusion(s32[1536]{0:T(1024)S(1)} %fusion.21, bf16[1536,512]{1,0:T(8,128)(2,1)S(1)} %reshape.100, bf16[]{:T(256)} %constant.8.clone.1), kind=kCustom, calls=%fused_computation.19 | custom fusion | bytes 3145730 | tf_op jit(solution)/shard_map/scatter | solution.py:44
  34.8 6.0 %all-to-all-start = ((bf16[8,384,512]{2,1,0:T(8,128)(2,1)}), bf16[8,384,512]{2,1,0:T(8,128)(2,1)S(1)}, u32[]{:S(2)}, u32[]{:S(2)}) async-start(bf16[8,384,512]{2,1,0:T(8,128)(2,1)} %bitcast.69), calls=%async_computation | async-start | bytes 6291456 | tf_op jit(solution)/shard_map/all_to_all | solution.py:52
  40.8 0.0 all-gather.11.cloned.1.call-start
  40.8 8.6 %all_gather.26 = bf16[1024,256]{1,0:T(8,128)(2,1)} all-gather(bf16[256,256]{1,0:T(8,128)(2,1)S(1)} %copy-done.2), channel_id=1, replica_groups=mesh['ep'=8,'tp'=4] {'tp'}, dimensions={0}, use_global_device_ids=true | all-gather | bytes 655360 | tf_op jit(solution)/shard_map/all_gather | solution.py:74
  49.5 0.0 all-gather.11.cloned.1.call-update
  49.5 75.0 %all-to-all-done = bf16[8,384,512]{2,1,0:T(8,128)(2,1)S(1)} async-done(((bf16[8,384,512]{2,1,0:T(8,128)(2,1)}), bf16[8,384,512]{2,1,0:T(8,128)(2,1)S(1)}, u32[]{:S(2)}, u32[]{:S(2)}) %all-to-all-start) | async-done | bytes 3145760 | tf_op jit(solution)/shard_map/all_to_all | solution.py:52
  124.5 39.5 %all_to_all.75 = bf16[8,384,512]{2,1,0:T(8,128)(2,1)S(1)} all-to-all(bf16[8,384,512]{2,1,0:T(8,128)(2,1)S(1)} %all-to-all-done), channel_id=1, replica_groups=mesh['ep'=8,'tp'=4] {'tp'}, dimensions={0} | all-to-all | bytes 6291456 | tf_op jit(solution)/shard_map/all_to_all | solution.py:51
  164.0 2.4 copy.32
  166.4 1.0 copy.41
  167.4 0.0 all-gather.13.cloned.1.call-done
  167.5 4.5 %fusion.3 = f32[768,512]{1,0:T(8,128)} fusion(bf16[768,2048]{1,0:T(8,128)(2,1)S(1)} %bitcast.73, bf16[1,2048,512]{2,1,0:T(8,128)(2,1)} %all-gather.13.cloned.1.call-done), kind=kOutput, calls=%fused_computation.8 | convolution fusion | flops 1610612736 | bytes 6815744 | tf_op jit(solution)/shard_map/dot_general | solution.py:59
  172.0 7.9 %convolution_convert_fusion = bf16[768,2048]{1,0:T(8,128)(2,1)} fusion(bf16[1,512,2048]{2,1,0:T(8,128)(2,1)} %all-gather.17.cloned.1.call-done, f32[768,512]{1,0:T(8,128)} %fusion.3, bf16[768,2048]{1,0:T(8,128)(2,1)S(1)} %bitcast.74, bf16[1,2048,512]{2,1,0:T(8,128)(2,1)} %all-gather.15.cloned.1.call-done), kind=kOutput, calls=%fused_computation.2 | convolution fusion | flops 3225157632 | bytes 12058624 | tf_op jit(solution)/shard_map/dot_general | solution.py:62
  179.9 8.8 %copy.33 = bf16[2,384,2048]{1,0,2:T(2,128)(2,1)} copy(bf16[2,384,2048]{2,1,0:T(8,128)(2,1)} %bitcast.75) | data formatting | bytes 6291456 | tf_op jit(solution)/shard_map/reshape | solution.py:64
  188.6 3.8 all-to-all-start.2
  192.5 0.0 all-gather.9.cloned.1.call-start
  192.5 0.0 copy-done.3
  192.5 40.9 %all_gather.24 = bf16[256,1024]{1,0:T(8,128)(2,1)} all-gather(bf16[256,256]{1,0:T(8,128)(2,1)S(1)} %copy-done.3), channel_id=1, replica_groups=mesh['ep'=8,'tp'=4] {'tp'}, dimensions={1}, use_global_device_ids=true | all-gather | bytes 655360 | tf_op jit(solution)/shard_map/all_gather | solution.py:73
  233.5 0.0 all-gather.9.cloned.1.call-update
  233.5 0.0 all-to-all-done.2
  233.5 4.2 %all-to-all-start.4 = ((bf16[4,192,512]{2,1,0:T(8,128)(2,1)}), bf16[4,192,512]{2,1,0:T(8,128)(2,1)}, u32[]{:S(2)}, u32[]{:S(2)}) async-start(bf16[4,192,512]{2,1,0:T(8,128)(2,1)} %bitcast.72), calls=%async_computation.4 | async-start | bytes 1572864 | tf_op jit(solution)/shard_map/all_to_all | solution.py:71
  237.7 6.7 %copy.34 = bf16[4,2,384,512]{3,2,1,0:T(8,128)(2,1)} copy(bf16[4,2,384,512]{2,1,3,0:T(2,128)(2,1)S(1)} %bitcast.68) | data formatting | bytes 6291456 | tf_op jit(solution)/shard_map/all_to_all | solution.py:63
  244.4 5.0 %all-to-all-done.4 = bf16[4,192,512]{2,1,0:T(8,128)(2,1)} async-done(((bf16[4,192,512]{2,1,0:T(8,128)(2,1)}), bf16[4,192,512]{2,1,0:T(8,128)(2,1)}, u32[]{:S(2)}, u32[]{:S(2)}) %all-to-all-start.4) | async-done | bytes 786464 | tf_op jit(solution)/shard_map/all_to_all | solution.py:71
  249.4 6.3 %all-to-all-start.3 = ((bf16[8,384,512]{2,1,0:T(8,128)(2,1)}), bf16[8,384,512]{2,1,0:T(8,128)(2,1)S(1)}, u32[]{:S(2)}, u32[]{:S(2)}) async-start(bf16[8,384,512]{2,1,0:T(8,128)(2,1)} %bitcast.67), calls=%async_computation.3 | async-start | bytes 6291456 | tf_op jit(solution)/shard_map/all_to_all | solution.py:13
  255.7 2.1 copy.39
  257.8 107.4 %all-gather.9.cloned.1.call-done = bf16[2048,1024]{1,0:T(8,128)(2,1)} async-done(((bf16[256,1024]{1,0:T(8,128)(2,1)}), bf16[2048,1024]{1,0:T(8,128)(2,1)}) %all-gather.9.cloned.1.call-update) | async-done | bytes 4194320 | tf_op jit(solution)/shard_map/all_gather | solution.py:77
  365.2 6.4 %convolution_convert_fusion.1 = bf16[192,2048]{1,0:T(8,128)(2,1)} fusion(bf16[1024,2048]{1,0:T(8,128)(2,1)} %all-gather.11.cloned.1.call-done, bf16[192,2048]{1,0:T(8,128)(2,1)} %bitcast.77, bf16[2048,1024]{1,0:T(8,128)(2,1)} %all-gather.9.cloned.1.call-done), kind=kOutput, calls=%fused_computation.4 | convolution fusion | flops 1611988992 | bytes 9961472 | tf_op jit(solution)/shard_map/dot_general | solution.py:83
  371.7 2.1 copy.44
  373.8 0.0 all-to-all-done.3
  373.8 4.4 %all-to-all-start.5 = ((bf16[192,4,512]{2,0,1:T(8,128)(2,1)}), bf16[192,4,512]{2,0,1:T(8,128)(2,1)}, u32[]{:S(2)}, u32[]{:S(2)}) async-start(bf16[192,4,512]{2,0,1:T(8,128)(2,1)} %bitcast.76), calls=%async_computation.5 | async-start | bytes 1572864 | tf_op jit(solution)/shard_map/all_to_all | solution.py:86
  378.2 0.0 copy-done.7
  378.2 0.6 add_divide_fusion
  378.8 0.2 copy.35
  379.0 5.4 %gather_fusion = bf16[1536,512]{1,0:T(8,128)(2,1)} fusion(bf16[3072,512]{1,0:T(8,128)(2,1)S(1)} %bitcast.66, s32[2048]{0:T(1024)S(1)} %pad_clamp_fusion), kind=kCustom, calls=%fused_computation | custom fusion | bytes 3151872 | tf_op jit(solution)/shard_map/gather | solution.py:67
  384.4 3.4 reshape.86
  387.8 5.9 %multiply_reduce_fusion = f32[768,512]{1,0:T(8,128)} fusion(f32[768,2,512]{2,1,0:T(2,128)S(1)} %reshape.86, f32[768,2]{1,0:T(8,128)S(1)} %copy.35), kind=kLoop, calls=%fused_computation.3 | loop fusion | flops 1179648 | bytes 4724736 | tf_op jit(solution)/shard_map/reduce_sum | solution.py:70
  393.7 0.0 all-to-all-done.5
  393.8 0.0 copy-done.4
  393.8 2.7 fusion.9
  (16 shorter events, 0.1 us)
Async XLA Ops:
  6.5 4.0 %copy-start.1 = (bf16[768,512]{1,0:T(8,128)(2,1)S(1)}, bf16[768,512]{1,0:T(8,128)(2,1)}, u32[]{:S(2)}) copy-start(bf16[768,512]{1,0:T(8,128)(2,1)} %param.10) | copy-start | bytes 2359300
  6.5 160.9 %all-gather.13.cloned.1.call-start = ((), (), s32[]{:S(2)}) async-start(), calls=%async_computation.8 | async-start | bytes 2621440 | tf_op jit(solution)/shard_map/all_gather | solution.py:47
  7.3 15.3 %copy-start.6 = (f32[512]{0:T(512)S(1)}, f32[512]{0:T(512)}, u32[]{:S(2)}) copy-start(f32[512]{0:T(512)} %param.11) | copy-start | bytes 6148
  7.3 164.7 %all-gather.15.cloned.1.call-start = ((), (), s32[]{:S(2)}) async-start(), calls=%async_computation.9 | async-start | bytes 2621440 | tf_op jit(solution)/shard_map/all_gather | solution.py:48
  8.0 164.0 %all-gather.17.cloned.1.call-start = ((), (), s32[]{:S(2)}) async-start(), calls=%async_computation.10 | async-start | bytes 2621440 | tf_op jit(solution)/shard_map/all_gather | solution.py:49
  22.9 0.9 copy-start
  34.8 6.0 %copy-start.2 = (bf16[256,256]{1,0:T(8,128)(2,1)S(1)}, bf16[256,256]{1,0:T(8,128)(2,1)}, u32[]{:S(2)}) copy-start(bf16[256,256]{1,0:T(8,128)(2,1)} %param.18) | copy-start | bytes 393220
  34.8 89.7 %all-to-all-start = ((bf16[8,384,512]{2,1,0:T(8,128)(2,1)}), bf16[8,384,512]{2,1,0:T(8,128)(2,1)S(1)}, u32[]{:S(2)}, u32[]{:S(2)}) async-start(bf16[8,384,512]{2,1,0:T(8,128)(2,1)} %bitcast.69), calls=%async_computation | async-start | bytes 6291456 | tf_op jit(solution)/shard_map/all_to_all | solution.py:52
  40.8 217.0 %all-gather.11.cloned.1.call-start = ((), (), s32[]{:S(2)}) async-start(), calls=%async_computation.7 | async-start | bytes 4718592 | tf_op jit(solution)/shard_map/all_gather | solution.py:78
  188.6 3.9 copy-start.3
  188.6 44.9 %all-to-all-start.2 = ((bf16[2,384,2048]{1,0,2:T(2,128)(2,1)}), bf16[2,384,2048]{1,0,2:T(2,128)(2,1)S(1)}, u32[]{:S(2)}, u32[]{:S(2)}) async-start(bf16[2,384,2048]{1,0,2:T(2,128)(2,1)} %copy.33), calls=%async_computation.2 | async-start | bytes 6291456 | tf_op jit(solution)/shard_map/all_to_all | solution.py:63
  192.5 172.7 %all-gather.9.cloned.1.call-start = ((), (), s32[]{:S(2)}) async-start(), calls=%async_computation.6 | async-start | bytes 4718592 | tf_op jit(solution)/shard_map/all_gather | solution.py:77
  233.5 15.9 %all-to-all-start.4 = ((bf16[4,192,512]{2,1,0:T(8,128)(2,1)}), bf16[4,192,512]{2,1,0:T(8,128)(2,1)}, u32[]{:S(2)}, u32[]{:S(2)}) async-start(bf16[4,192,512]{2,1,0:T(8,128)(2,1)} %bitcast.72), calls=%async_computation.4 | async-start | bytes 1572864 | tf_op jit(solution)/shard_map/all_to_all | solution.py:71
  249.4 124.4 %all-to-all-start.3 = ((bf16[8,384,512]{2,1,0:T(8,128)(2,1)}), bf16[8,384,512]{2,1,0:T(8,128)(2,1)S(1)}, u32[]{:S(2)}, u32[]{:S(2)}) async-start(bf16[8,384,512]{2,1,0:T(8,128)(2,1)} %bitcast.67), calls=%async_computation.3 | async-start | bytes 6291456 | tf_op jit(solution)/shard_map/all_to_all | solution.py:13
  371.7 6.6 %copy-start.7 = (f32[512]{0:T(512)S(1)}, f32[512]{0:T(512)}, u32[]{:S(2)}) copy-start(f32[512]{0:T(512)} %param.19) | copy-start | bytes 6148
  371.7 7.2 %copy-start.5 = (f32[768,2]{0,1:T(2,128)S(1)}, f32[768,2]{0,1:T(2,128)}, u32[]{:S(2)}) copy-start(f32[768,2]{0,1:T(2,128)} %param.13) | copy-start | bytes 18436
  373.8 20.0 %all-to-all-start.5 = ((bf16[192,4,512]{2,0,1:T(8,128)(2,1)}), bf16[192,4,512]{2,0,1:T(8,128)(2,1)}, u32[]{:S(2)}, u32[]{:S(2)}) async-start(bf16[192,4,512]{2,0,1:T(8,128)(2,1)} %bitcast.76), calls=%async_computation.5 | async-start | bytes 1572864 | tf_op jit(solution)/shard_map/all_to_all | solution.py:86
  387.8 5.9 %copy-start.4 = (f32[512]{0:T(512)S(1)}, f32[512]{0:T(512)}, u32[]{:S(2)}) copy-start(f32[512]{0:T(512)} %add_divide_fusion) | copy-start | bytes 6148
Sparse Core Ops, SparseCore 0:
  8.9 25.2 all-gather.12
  35.8 23.4 all-gather.14
  60.8 23.6 all-gather.16
  86.4 92.0 all-gather.10
  233.6 131.5 all-gather.8
where the time goes:
time: 404 us; the launch traced here: 403 us
  waiting for transfers between devices  190 us (47%)
  blocking collectives  97.4 us (24%)
  local copies, waits for them, and re-layouts  46 us (11%)
  starting transfers between devices  24.9 us (6%)
  matrix products  18.9 us (5%)
  between operations  13.4 us (3%)
  other arithmetic  13 us (3%)
    all_gather x1, waiting for transfers between devices, body(): lax.all_gather(in_cols, 'ep', axis=0, tiled=True)  107 us
    all_to_all x1, waiting for transfers between devices, body(): lax.all_to_all(buffer, 'ep', split_axis=0, concat_axis=0, tiled=True)  75 us
    all_gather x1, blocking collectives, body(): lax.all_gather(w_branch_in, 'tp', axis=1, tiled=True)  40.9 us
    all_to_all x1, blocking collectives, body(): lax.all_to_all(lax.all_to_all(buffer, 'ep', split_axis=0, concat_axis=0,...  39.5 us
    scatter x1, local copies, waits for them, and re-layouts, body(): jnp.zeros((expert_count * capacity, quarter), jnp.bfloat16).at[position]  9.46 us
    reshape x1, local copies, waits for them, and re-layouts, body(): result.reshape(row_split.shape)  8.75 us
    all_gather x1, blocking collectives, body(): lax.all_gather(w_branch_out, 'tp', axis=0, tiled=True)  8.6 us
    psum x1, blocking collectives, body(): squares = lax.psum(jnp.sum(floats * floats, axis=1), 'tp')  8.37 us
  transfers between devices with their start and end apart: 10, of which 3 were waited for; matrix products, arithmetic and copies ran while one was open for 18% of the time, Pallas kernels for 0%

commit v1 on v0

--- a/solution.py
+++ b/solution.py
@@ -1,6 +1,10 @@
+import functools
+
 import jax
 import jax.numpy as jnp
 from jax import lax
+from jax.experimental import pallas as pl
+from jax.experimental.pallas import tpu as pltpu
 from jax.sharding import PartitionSpec as P
 
 GROUPS = 4
@@ -87,9 +91,405 @@
     return (routed + jax.nn.sigmoid(branch_gate) * branch.astype(jnp.float32)).astype(jnp.bfloat16)
 
 
+BF16, F32 = jnp.bfloat16, jnp.float32
+COPIES = 47
+
+
+def dot(a, b):
+    return jnp.dot(a, b, preferred_element_type=F32)
+
+
+def dot_nt(a, b):
+    return lax.dot_general(a, b, (((1,), (1,)), ((), ())), preferred_element_type=F32)
+
+
+def silu(v):
+    return v / (1.0 + jnp.exp(-v))
+
+
+def pair_kernel(
+    tokens,
+    gain,
+    routing,
+    route_weight,
+    w_gate,
+    w_up,
+    w_down,
+    w_in,
+    w_out,
+    branch_gate,
+    out,
+    gate_y,
+    up_y,
+    down_y,
+    gate_s,
+    up_s,
+    down_s,
+    squares,
+    normed,
+    in_all,
+    out_all,
+    slots_out,
+    slots,
+    slots_s,
+    scale_out,
+    scale,
+    part_out,
+    part_own,
+    part_in,
+    hidden,
+    half_out,
+    half_own,
+    half_in,
+    back_out,
+    back,
+    fold_out,
+    fold_own,
+    fold_in,
+    cross_out,
+    cross_in,
+    branch_hidden,
+    code_col,
+    send_sem,
+    recv_sem,
+):
+    ep, tp = lax.axis_index("ep"), lax.axis_index("tp")
+    z, y, x, c = ep // 2, ep % 2, tp // 2, tp % 2
+    token_count, quarter = tokens.shape
+    ff = w_gate.shape[1]
+    capacity = slots.shape[1]
+    half = capacity // 2
+    block = w_in.shape[0]
+
+    def at(zz, yy, xx, cc):
+        return (zz * 2 + yy, xx * 2 + cc)
+
+    sibling = at(z, y, x, 1 - c)
+    across = at(z, y, 1 - x, c)
+    diagonal = at(z, y, 1 - x, 1 - c)
+    pair = at(z, 1 - y, x, c)
+    ahead = [None] + [at((z + s) % GROUPS, y, x, c) for s in range(1, GROUPS)]
+    behind = [None] + [at((z + GROUPS - s) % GROUPS, y, x, c) for s in range(1, GROUPS)]
+
+    barrier = pltpu.get_barrier_semaphore()
+    peers = [sibling, across, diagonal, pair] + ahead[1:]
+    for peer in peers:
+        pl.semaphore_signal(
+            barrier, inc=1, device_id=peer, device_id_type=pl.DeviceIdType.MESH
+        )
+    pl.semaphore_wait(barrier, len(peers))
+
+    started = {}
+
+    def send(number, source, target, device):
+        copy = pltpu.make_async_remote_copy(
+            src_ref=source,
+            dst_ref=target,
+            send_sem=send_sem.at[number],
+            recv_sem=recv_sem.at[number],
+            device_id=device,
+            device_id_type=pl.DeviceIdType.MESH,
+        )
+        copy.start()
+        started[number] = copy
+
+    def arrived(number):
+        started[number].wait_recv()
+
+    send(0, w_gate, gate_y.at[y], pair)
+    send(1, w_up, up_y.at[y], pair)
+    send(2, w_down, down_y.at[y], pair)
+
+    floats = tokens[...].astype(F32)
+    exact = floats * floats
+    high = exact.astype(BF16)
+    low = (exact - high.astype(F32)).astype(BF16)
+    ones = jnp.ones((16, quarter), BF16)
+    squares[0] = (dot_nt(ones, high) + dot_nt(ones, low))[:8]
+    send(6, squares.at[0], squares.at[1], sibling)
+    send(7, squares.at[0], squares.at[2], across)
+    send(8, squares.at[0], squares.at[3], diagonal)
+
+    for s in range(1, GROUPS):
+        send(11 + s, w_in, in_all.at[y, z], ahead[s])
+        send(14 + s, w_out, out_all.at[y, z], ahead[s])
+    in_all[y, z] = w_in[...]
+    out_all[y, z] = w_out[...]
+    gate_y[y] = w_gate[...]
+    up_y[y] = w_up[...]
+    down_y[y] = w_down[...]
+
+    ids = routing[0:1, :]
+    group = lax.shift_right_logical(ids, 1)
+    rows16 = lax.broadcasted_iota(jnp.int32, (16, token_count), 0)
+    member = jnp.where(rows16 == group, 1.0, 0.0)
+    earlier = jnp.where(
+        lax.broadcasted_iota(jnp.int32, (token_count, token_count), 0)
+        < lax.broadcasted_iota(jnp.int32, (token_count, token_count), 1),
+        1.0,
+        0.0,
+    ).astype(BF16)
+    before = dot(member.astype(BF16), earlier)
+    place = jnp.sum(member * before, axis=0, keepdims=True)
+    code = group.astype(F32) * capacity + place
+    code_col[...] = jnp.transpose(jnp.broadcast_to(code, (8, token_count)))
+    first, second = route_weight[0:1, :], route_weight[1:2, :]
+    even_first = (ids & 1) == 0
+    for_even = jnp.where(even_first, first, second)
+    for_odd = jnp.where(even_first, second, first)
+    weights = jnp.where((rows16 & 1) == 0, for_even, for_odd)
+    weights_high = weights.astype(BF16)
+    weights_low = (weights - weights_high.astype(F32)).astype(BF16)
+
+    for number in (6, 7, 8):
+        arrived(number)
+    total = squares[0] + squares[1] + squares[2] + squares[3]
+    factor = lax.rsqrt(total / (4 * quarter) + epsilon)
+    factor_col = jnp.transpose(factor)[:, 0:1]
+    normed[0] = (tokens[...].astype(F32) * factor_col * gain[...]).astype(BF16)
+    send(9, normed.at[0], normed.at[1], sibling)
+
+    slot_row = lax.broadcasted_iota(jnp.int32, (capacity, token_count), 0)
+    for s in (2, 1, 3, 0):
+        wanted = (slot_row + ((z + s) % GROUPS) * capacity).astype(F32)
+        choose = jnp.where(wanted == code, 1.0, 0.0).astype(BF16)
+        rows = dot(choose, normed[0]).astype(BF16)
+        slot_weights = (dot_nt(weights_high, choose) + dot_nt(weights_low, choose))[:8]
+        if s == 0:
+            slots[0] = rows
+            scale[0] = slot_weights
+            send(26, slots.at[0], slots_s.at[0], sibling)
+        else:
+            slots_out[s] = rows
+            scale_out[s] = slot_weights
+            send(19 + s, slots_out.at[s], slots.at[s], ahead[s])
+            send(22 + s, scale_out.at[s], scale.at[s], ahead[s])
+    send(10, normed.at[0], normed.at[2], across)
+
+    def share(number, stage):
+        arrived(number)
+        whole, rest = stage
+        send(number + 3, whole.at[1 - c], rest, sibling)
+
+    def project(s, start):
+        own = slots[s, pl.ds(start, half), :]
+        other = slots_s[s, pl.ds(start, half), :]
+        return (
+            dot(own, gate_y[c]) + dot(other, gate_s[...]),
+            dot(own, up_y[c]) + dot(other, up_s[...]),
+        )
+
+    mine = pl.multiple_of(x * half, half)
+    theirs = pl.multiple_of((1 - x) * half, half)
+
+    def forward(s):
+        if s:
+            arrived(19 + s)
+            send(26 + s, slots.at[s], slots_s.at[s], sibling)
+
+    def stage_a(s):
+        arrived(26 + s)
+        gate_part, up_part = project(s, theirs)
+        part_out[s, :, :ff] = gate_part.astype(BF16)
+        part_out[s, :, ff:] = up_part.astype(BF16)
+        send(30 + s, part_out.at[s], part_in.at[s], across)
+        gate_part, up_part = project(s, mine)
+        part_own[s, :, :ff] = gate_part
+        part_own[s, :, ff:] = up_part
+
+    def stage_b(s):
+        arrived(30 + s)
+        gate_sum = part_own[s, :, :ff] + part_in[s, :, :ff].astype(F32)
+        up_sum = part_own[s, :, ff:] + part_in[s, :, ff:].astype(F32)
+        hidden[s, pl.ds(mine, half), :] = (silu(gate_sum) * up_sum).astype(BF16)
+        kept = hidden.at[s, pl.ds(mine, half), :]
+        send(34 + s, kept, kept, across)
+
+    def stage_c(s):
+        arrived(34 + s)
+        if s:
+            arrived(22 + s)
+        columns = jnp.transpose(scale[s])
+        weight = jnp.where(c == 0, columns[:, 0:1], columns[:, 1:2])
+        units = hidden[s]
+        half_out[s] = (dot(units, down_s[...]) * weight).astype(BF16)
+        send(38 + s, half_out.at[s], half_in.at[s], sibling)
+        half_own[s] = dot(units, down_y[c]) * weight
+
+    def stage_d(s):
+        arrived(38 + s)
+        both = (half_own[s] + half_in[s].astype(F32)).astype(BF16)
+        if s == 0:
+            back[0] = both
+        else:
+            back_out[s] = both
+            send(41 + s, back_out.at[s], back.at[s], behind[s])
+
+    share(0, (gate_y, gate_s))
+    share(1, (up_y, up_s))
+    arrived(3)
+    arrived(4)
+    stage_a(0)
+    forward(1)
+    arrived(10)
+    send(11, normed.at[2], normed.at[3], sibling)
+    stage_a(1)
+    share(2, (down_y, down_s))
+    for s in range(1, GROUPS):
+        arrived(11 + s)
+        arrived(14 + s)
+    send(18, in_all.at[y], in_all.at[y], pair)
+    send(19, out_all.at[y], out_all.at[y], pair)
+    stage_b(0)
+    order = (0, 1, 3, 2)
+    forward(order[2])
+    stage_a(order[2])
+    stage_b(1)
+    arrived(5)
+    stage_c(0)
+    forward(order[3])
+    stage_a(order[3])
+    stage_d(0)
+    stage_c(1)
+    stage_b(order[2])
+    stage_d(1)
+
+    arrived(9)
+    arrived(11)
+    arrived(18)
+    quarters = (tp, x * 2 + 1 - c, (1 - x) * 2 + c, (1 - x) * 2 + 1 - c)
+    sums = jnp.zeros((token_count, block), F32)
+    for k, q in enumerate(quarters):
+        sums = sums + dot(normed[k, :, :block], in_all[0, q])
+        sums = sums + dot(normed[k, :, block:], in_all[1, q])
+    branch_hidden[...] = silu(sums).astype(BF16)
+    arrived(19)
+
+    def branch_part(q, side):
+        return dot(branch_hidden[...], out_all[side, q])
+
+    for side in range(2):
+        columns = slice(side * block, (side + 1) * block)
+        fold_out[0, :, columns] = branch_part(quarters[1], side).astype(BF16)
+        fold_out[1, :, columns] = branch_part(quarters[3], side).astype(BF16)
+    send(45, fold_out, fold_in, sibling)
+
+    stage_c(order[2])
+    stage_b(order[3])
+    stage_d(order[2])
+
+    arrived(45)
+    for side in range(2):
+        columns = slice(side * block, (side + 1) * block)
+        cross_out[:, columns] = (
+            branch_part(quarters[2], side) + fold_in[1, :, columns].astype(F32)
+        ).astype(BF16)
+    stage_c(order[3])
+    send(46, cross_out, cross_in, across)
+    stage_d(order[3])
+    for side in range(2):
+        columns = slice(side * block, (side + 1) * block)
+        fold_own[:, columns] = branch_part(quarters[0], side) + fold_in[0, :, columns].astype(F32)
+
+    slot_lane = lax.broadcasted_iota(jnp.int32, (token_count, capacity), 1)
+
+    def restore(s):
+        wanted = (slot_lane + ((z + s) % GROUPS) * capacity).astype(F32)
+        choose = jnp.where(wanted == code_col[:, 0:1], 1.0, 0.0).astype(BF16)
+        return dot(choose, back[s])
+
+    half_own_sum = restore(0)
+    for s in (1,) + order[2:]:
+        arrived(41 + s)
+        half_own_sum = half_own_sum + restore(s)
+    arrived(46)
+    branch = fold_own[...] + cross_in[...].astype(F32)
+    gate = 1.0 / (1.0 + jnp.exp(-branch_gate[...]))
+    out[...] = (half_own_sum + gate * branch).astype(BF16)
+    for copy in started.values():
+        copy.wait_send()
+
+
+def pair_body(
+    tokens,
+    norm_gain,
+    routing,
+    route_weight,
+    w_gate,
+    w_up,
+    w_down,
+    w_branch_in,
+    w_branch_out,
+    branch_gate,
+):
+    count, quarter = tokens.shape
+    ff = w_gate.shape[2]
+    block = w_branch_in.shape[0]
+    cap = count // 2
+    half = cap // 2
+    vmem = pltpu.VMEM
+    rows = (GROUPS, cap, quarter)
+    scratch = [
+        vmem((2, quarter, ff), BF16),
+        vmem((2, quarter, ff), BF16),
+        vmem((2, ff, quarter), BF16),
+        vmem((quarter, ff), BF16),
+        vmem((quarter, ff), BF16),
+        vmem((ff, quarter), BF16),
+        vmem((4, 8, count), F32),
+        vmem((4, count, quarter), BF16),
+        vmem((2, GROUPS, block, block), BF16),
+        vmem((2, GROUPS, block, block), BF16),
+        vmem(rows, BF16),
+        vmem(rows, BF16),
+        vmem(rows, BF16),
+        vmem((GROUPS, 8, cap), F32),
+        vmem((GROUPS, 8, cap), F32),
+        vmem((GROUPS, half, 2 * ff), BF16),
+        vmem((GROUPS, half, 2 * ff), F32),
+        vmem((GROUPS, half, 2 * ff), BF16),
+        vmem((GROUPS, cap, ff), BF16),
+        vmem(rows, BF16),
+        vmem(rows, F32),
+        vmem(rows, BF16),
+        vmem(rows, BF16),
+        vmem(rows, BF16),
+        vmem((2, count, quarter), BF16),
+        vmem((count, quarter), F32),
+        vmem((2, count, quarter), BF16),
+        vmem((count, quarter), BF16),
+        vmem((count, quarter), BF16),
+        vmem((count, block), BF16),
+        vmem((count, 8), F32),
+        pltpu.SemaphoreType.DMA((COPIES,)),
+        pltpu.SemaphoreType.DMA((COPIES,)),
+    ]
+    return pl.pallas_call(
+        pair_kernel,
+        out_shape=jax.ShapeDtypeStruct((count, quarter), BF16),
+        in_specs=[pl.BlockSpec(memory_space=vmem)] * 10,
+        out_specs=pl.BlockSpec(memory_space=vmem),
+        scratch_shapes=scratch,
+        compiler_params=pltpu.CompilerParams(
+            collective_id=0, has_side_effects=True, vmem_limit_bytes=60 * 1024 * 1024
+        ),
+    )(
+        tokens,
+        norm_gain[None, :],
+        routing.T,
+        route_weight.T,
+        w_gate[0],
+        w_up[0],
+        w_down[0],
+        w_branch_in,
+        w_branch_out,
+        branch_gate[None, :],
+    )
+
+
 def solution(mesh):
     return jax.shard_map(
-        body,
+        pair_body if mesh.shape["ep"] == 2 * GROUPS and mesh.shape["tp"] == 4 else body,
         mesh=mesh,
         in_specs=(
             P("ep", "tp"),

time: 404 us -> 136 us (0.34)
  the two profiles are of different devices: /device:TPU:0 before, /device:TPU:21 now
where the time goes in v1:
time: 136 us; the launch traced here: 135 us
  Pallas kernels  133 us (98%)
  local copies, waits for them, and re-layouts  2.06 us (2%)
    pallas_call x1, Pallas kernels, pair_body(): pl.pallas_call(pair_kernel, out_shape=jax.ShapeDtypeStruct((count, quarte...  133 us

profile of v1, /device:TPU:21, one launch (start us, length us, event | category | flops | bytes accessed | tf_op | source)
XLA Modules:
  0.0 135.5 jit_solution(5985385002460995194)
XLA Ops:
  0.0 133.4 %shard_map.100 = bf16[768,512]{1,0:T(8,128)(2,1)} custom-call(bf16[768,512]{1,0:T(8,128)(2,1)} %tokens.1, f32[1,512]{1,0:T(1,128)} %bitcast.12, s32[2,768]{1,0:T(2,128)} %bitcast.10, f32[2,768]{1,0:T(2,128)} %bitcast.11, bf16[512,512]{1,0:T(8,128)(2,1)} %bitcast.7, bf16[512,512]{1,0:T(8,128)(2,1)} %bitcast.8, bf16[512,512]{1,0:T(8,128)(2,1)} %bitcast.9, ...), custom_call_target="tpu_custom_call" | custom-call | tf_op jit(solution)/shard_map/pallas_call | solution.py:467
  133.4 2.1 %copy.12 = bf16[768,512]{1,0:T(8,128)(2,1)} copy(bf16[768,512]{1,0:T(8,128)(2,1)} %shard_map.100) | data formatting | bytes 1572864

commit v2 on v1

--- a/solution.py
+++ b/solution.py
@@ -92,7 +92,7 @@
 
 
 BF16, F32 = jnp.bfloat16, jnp.float32
-COPIES = 47
+COPIES = 53
 
 
 def dot(a, b):
@@ -127,8 +127,7 @@
     down_s,
     squares,
     normed,
-    in_all,
-    out_all,
+    branch_all,
     slots_out,
     slots,
     slots_s,
@@ -168,15 +167,27 @@
     across = at(z, y, 1 - x, c)
     diagonal = at(z, y, 1 - x, 1 - c)
     pair = at(z, 1 - y, x, c)
-    ahead = [None] + [at((z + s) % GROUPS, y, x, c) for s in range(1, GROUPS)]
-    behind = [None] + [at((z + GROUPS - s) % GROUPS, y, x, c) for s in range(1, GROUPS)]
+    level = [z, z + 1 - 2 * (z % 2), (z + 2) % GROUPS, GROUPS - 1 - z]
+    peer_of = [None] + [at(level[m], y, x, c) for m in range(1, GROUPS)]
+    up = at((z + 1) % GROUPS, y, x, c)
+    down = at((z + GROUPS - 1) % GROUPS, y, x, c)
 
     barrier = pltpu.get_barrier_semaphore()
-    peers = [sibling, across, diagonal, pair] + ahead[1:]
+    peers = [sibling, across, diagonal, pair] + peer_of[1:]
     for peer in peers:
         pl.semaphore_signal(
             barrier, inc=1, device_id=peer, device_id_type=pl.DeviceIdType.MESH
         )
+
+    branch_all[y, z, 0] = w_in[...]
+    branch_all[y, z, 1] = w_out[...]
+    floats = tokens[...].astype(F32)
+    exact = floats * floats
+    high = exact.astype(BF16)
+    low = (exact - high.astype(F32)).astype(BF16)
+    ones = jnp.ones((16, quarter), BF16)
+    squares[0] = (dot_nt(ones, high) + dot_nt(ones, low))[:8]
+
     pl.semaphore_wait(barrier, len(peers))
 
     started = {}
@@ -196,25 +207,62 @@
     def arrived(number):
         started[number].wait_recv()
 
+    send(6, squares.at[0], squares.at[1], sibling)
+    send(7, squares.at[0], squares.at[2], across)
+    send(8, squares.at[0], squares.at[3], diagonal)
+
     send(0, w_gate, gate_y.at[y], pair)
     send(1, w_up, up_y.at[y], pair)
     send(2, w_down, down_y.at[y], pair)
 
-    floats = tokens[...].astype(F32)
-    exact = floats * floats
-    high = exact.astype(BF16)
-    low = (exact - high.astype(F32)).astype(BF16)
-    ones = jnp.ones((16, quarter), BF16)
-    squares[0] = (dot_nt(ones, high) + dot_nt(ones, low))[:8]
-    send(6, squares.at[0], squares.at[1], sibling)
-    send(7, squares.at[0], squares.at[2], across)
-    send(8, squares.at[0], squares.at[3], diagonal)
-
-    for s in range(1, GROUPS):
-        send(11 + s, w_in, in_all.at[y, z], ahead[s])
-        send(14 + s, w_out, out_all.at[y, z], ahead[s])
-    in_all[y, z] = w_in[...]
-    out_all[y, z] = w_out[...]
+    def relay(hop, upward):
+        number = (12 if upward else 47) + hop - 1
+        held = z - (hop - 1) if upward else z + (hop - 1)
+        came = z - hop if upward else z + hop
+        held, came = (held + GROUPS) % GROUPS, (came + GROUPS) % GROUPS
+        sends = (z <= GROUPS - 2) & (z >= hop - 1)
+        gets = z >= hop
+        if not upward:
+            sends = (z >= 1) & (z <= GROUPS - hop)
+            gets = z <= GROUPS - 1 - hop
+
+        def copy(row):
+            return pltpu.make_async_remote_copy(
+                src_ref=branch_all.at[y, row],
+                dst_ref=branch_all.at[y, row],
+                send_sem=send_sem.at[number],
+                recv_sem=recv_sem.at[number],
+                device_id=up if upward else down,
+                device_id_type=pl.DeviceIdType.MESH,
+            )
+
+        return sends, gets, lambda: copy(held), lambda: copy(came)
+
+    def relay_start(hop):
+        for upward in (True, False):
+            sends, _, outgoing, _ = relay(hop, upward)
+
+            @pl.when(sends)
+            def _():
+                outgoing().start()
+
+    def relay_arrived(hop):
+        for upward in (True, False):
+            _, gets, _, incoming = relay(hop, upward)
+
+            @pl.when(gets)
+            def _():
+                incoming().wait_recv()
+
+    def relay_sent(hop):
+        for upward in (True, False):
+            sends, _, outgoing, _ = relay(hop, upward)
+
+            @pl.when(sends)
+            def _():
+                outgoing().wait_send()
+
+    relay_start(1)
     gate_y[y] = w_gate[...]
     up_y[y] = w_up[...]
     down_y[y] = w_down[...]
@@ -247,11 +295,14 @@
     factor = lax.rsqrt(total / (4 * quarter) + epsilon)
     factor_col = jnp.transpose(factor)[:, 0:1]
     normed[0] = (tokens[...].astype(F32) * factor_col * gain[...]).astype(BF16)
+    send(10, normed.at[0], normed.at[2], across)
     send(9, normed.at[0], normed.at[1], sibling)
+    relay_arrived(1)
+    relay_start(2)
 
     slot_row = lax.broadcasted_iota(jnp.int32, (capacity, token_count), 0)
-    for s in (2, 1, 3, 0):
-        wanted = (slot_row + ((z + s) % GROUPS) * capacity).astype(F32)
+    for s in (2, 3, 1, 0):
+        wanted = (slot_row + level[s] * capacity).astype(F32)
         choose = jnp.where(wanted == code, 1.0, 0.0).astype(BF16)
         rows = dot(choose, normed[0]).astype(BF16)
         slot_weights = (dot_nt(weights_high, choose) + dot_nt(weights_low, choose))[:8]
@@ -262,9 +313,8 @@
         else:
             slots_out[s] = rows
             scale_out[s] = slot_weights
-            send(19 + s, slots_out.at[s], slots.at[s], ahead[s])
-            send(22 + s, scale_out.at[s], scale.at[s], ahead[s])
-    send(10, normed.at[0], normed.at[2], across)
+            send(19 + s, slots_out.at[s], slots.at[s], peer_of[s])
+            send(22 + s, scale_out.at[s], scale.at[s], peer_of[s])
 
     def share(number, stage):
         arrived(number)
@@ -323,36 +373,34 @@
             back[0] = both
         else:
             back_out[s] = both
-            send(41 + s, back_out.at[s], back.at[s], behind[s])
+            send(41 + s, back_out.at[s], back.at[s], peer_of[s])
 
     share(0, (gate_y, gate_s))
+    relay_arrived(2)
+    relay_start(3)
+    forward(2)
     share(1, (up_y, up_s))
     arrived(3)
     arrived(4)
+    stage_a(2)
     stage_a(0)
-    forward(1)
     arrived(10)
     send(11, normed.at[2], normed.at[3], sibling)
+    share(2, (down_y, down_s))
+    relay_arrived(3)
+    send(18, branch_all.at[y], branch_all.at[y], pair)
+    stage_b(2)
+    forward(3)
+    stage_a(3)
+    stage_b(0)
+    arrived(5)
+    stage_c(2)
+    stage_d(2)
+    forward(1)
     stage_a(1)
-    share(2, (down_y, down_s))
-    for s in range(1, GROUPS):
-        arrived(11 + s)
-        arrived(14 + s)
-    send(18, in_all.at[y], in_all.at[y], pair)
-    send(19, out_all.at[y], out_all.at[y], pair)
-    stage_b(0)
-    order = (0, 1, 3, 2)
-    forward(order[2])
-    stage_a(order[2])
-    stage_b(1)
-    arrived(5)
+    stage_b(3)
     stage_c(0)
-    forward(order[3])
-    stage_a(order[3])
     stage_d(0)
-    stage_c(1)
-    stage_b(order[2])
-    stage_d(1)
 
     arrived(9)
     arrived(11)
@@ -360,13 +408,12 @@
     quarters = (tp, x * 2 + 1 - c, (1 - x) * 2 + c, (1 - x) * 2 + 1 - c)
     sums = jnp.zeros((token_count, block), F32)
     for k, q in enumerate(quarters):
-        sums = sums + dot(normed[k, :, :block], in_all[0, q])
-        sums = sums + dot(normed[k, :, block:], in_all[1, q])
+        sums = sums + dot(normed[k, :, :block], branch_all[0, q, 0])
+        sums = sums + dot(normed[k, :, block:], branch_all[1, q, 0])
     branch_hidden[...] = silu(sums).astype(BF16)
-    arrived(19)
 
     def branch_part(q, side):
-        return dot(branch_hidden[...], out_all[side, q])
+        return dot(branch_hidden[...], branch_all[side, q, 1])
 
     for side in range(2):
         columns = slice(side * block, (side + 1) * block)
@@ -374,9 +421,9 @@
         fold_out[1, :, columns] = branch_part(quarters[3], side).astype(BF16)
     send(45, fold_out, fold_in, sibling)
 
-    stage_c(order[2])
-    stage_b(order[3])
-    stage_d(order[2])
+    stage_b(1)
+    stage_c(3)
+    stage_d(3)
 
     arrived(45)
     for side in range(2):
@@ -384,9 +431,9 @@
         cross_out[:, columns] = (
             branch_part(quarters[2], side) + fold_in[1, :, columns].astype(F32)
         ).astype(BF16)
-    stage_c(order[3])
     send(46, cross_out, cross_in, across)
-    stage_d(order[3])
+    stage_c(1)
+    stage_d(1)
     for side in range(2):
         columns = slice(side * block, (side + 1) * block)
         fold_own[:, columns] = branch_part(quarters[0], side) + fold_in[0, :, columns].astype(F32)
@@ -394,12 +441,12 @@
     slot_lane = lax.broadcasted_iota(jnp.int32, (token_count, capacity), 1)
 
     def restore(s):
-        wanted = (slot_lane + ((z + s) % GROUPS) * capacity).astype(F32)
+        wanted = (slot_lane + level[s] * capacity).astype(F32)
         choose = jnp.where(wanted == code_col[:, 0:1], 1.0, 0.0).astype(BF16)
         return dot(choose, back[s])
 
     half_own_sum = restore(0)
-    for s in (1,) + order[2:]:
+    for s in (2, 3, 1):
         arrived(41 + s)
         half_own_sum = half_own_sum + restore(s)
     arrived(46)
@@ -408,6 +455,8 @@
     out[...] = (half_own_sum + gate * branch).astype(BF16)
     for copy in started.values():
         copy.wait_send()
+    for hop in range(1, GROUPS):
+        relay_sent(hop)
 
 
 def pair_body(
@@ -438,8 +487,7 @@
         vmem((ff, quarter), BF16),
         vmem((4, 8, count), F32),
         vmem((4, count, quarter), BF16),
-        vmem((2, GROUPS, block, block), BF16),
-        vmem((2, GROUPS, block, block), BF16),
+        vmem((2, GROUPS, 2, block, block), BF16),
         vmem(rows, BF16),
         vmem(rows, BF16),
         vmem(rows, BF16),

time: 136 us -> 124 us (0.912)
  the two profiles are of different devices: /device:TPU:21 before, /device:TPU:0 now
where the time goes in v2:
time: 124 us
  Pallas kernels  122 us (98%)
  local copies, waits for them, and re-layouts  2.06 us (2%)
    pallas_call x1, Pallas kernels, pair_body(): pl.pallas_call(pair_kernel, out_shape=jax.ShapeDtypeStruct((count, quarte...  122 us

profile of v2, /device:TPU:0, one launch (start us, length us, event | category | flops | bytes accessed | tf_op | source)
XLA Modules:
  0.0 123.9 jit_solution(12017383774586980712)
XLA Ops:
  0.0 121.8 %shard_map.100 = bf16[768,512]{1,0:T(8,128)(2,1)} custom-call(bf16[768,512]{1,0:T(8,128)(2,1)} %tokens.1, f32[1,512]{1,0:T(1,128)} %bitcast.12, s32[2,768]{1,0:T(2,128)} %bitcast.10, f32[2,768]{1,0:T(2,128)} %bitcast.11, bf16[512,512]{1,0:T(8,128)(2,1)} %bitcast.7, bf16[512,512]{1,0:T(8,128)(2,1)} %bitcast.8, bf16[512,512]{1,0:T(8,128)(2,1)} %bitcast.9, ...), custom_call_target="tpu_custom_call" | custom-call | tf_op jit(solution)/shard_map/pallas_call | solution.py:515
  121.8 2.1 %copy.12 = bf16[768,512]{1,0:T(8,128)(2,1)} copy(bf16[768,512]{1,0:T(8,128)(2,1)} %shard_map.100) | data formatting | bytes 1572864

commit v3 on v2

--- a/solution.py
+++ b/solution.py
@@ -119,12 +119,9 @@
     w_out,
     branch_gate,
     out,
-    gate_y,
-    up_y,
-    down_y,
-    gate_s,
-    up_s,
-    down_s,
+    gate_all,
+    up_all,
+    down_all,
     squares,
     normed,
     branch_all,
@@ -167,13 +164,15 @@
     across = at(z, y, 1 - x, c)
     diagonal = at(z, y, 1 - x, 1 - c)
     pair = at(z, 1 - y, x, c)
+    pair_user = at(z, 1 - y, x, y)
+    pair_other = at(z, 1 - y, x, 1 - c)
     level = [z, z + 1 - 2 * (z % 2), (z + 2) % GROUPS, GROUPS - 1 - z]
     peer_of = [None] + [at(level[m], y, x, c) for m in range(1, GROUPS)]
     up = at((z + 1) % GROUPS, y, x, c)
     down = at((z + GROUPS - 1) % GROUPS, y, x, c)
 
     barrier = pltpu.get_barrier_semaphore()
-    peers = [sibling, across, diagonal, pair] + peer_of[1:]
+    peers = [sibling, across, diagonal, pair, pair_other] + peer_of[1:]
     for peer in peers:
         pl.semaphore_signal(
             barrier, inc=1, device_id=peer, device_id_type=pl.DeviceIdType.MESH
@@ -211,9 +210,50 @@
     send(7, squares.at[0], squares.at[2], across)
     send(8, squares.at[0], squares.at[3], diagonal)
 
-    send(0, w_gate, gate_y.at[y], pair)
-    send(1, w_up, up_y.at[y], pair)
-    send(2, w_down, down_y.at[y], pair)
+    weights_of = ((w_gate, gate_all), (w_up, up_all), (w_down, down_all))
+
+    def weight_copy(k, sem, device):
+        source, target = weights_of[k]
+        return pltpu.make_async_remote_copy(
+            src_ref=source,
+            dst_ref=target.at[c],
+            send_sem=send_sem.at[2 * k + sem],
+            recv_sem=recv_sem.at[2 * k + c],
+            device_id=device,
+            device_id_type=pl.DeviceIdType.MESH,
+        )
+
+    for k in range(3):
+        weight_copy(k, 0, pair_user).start()
+
+    @pl.when(c != y)
+    def _():
+        for k in range(3):
+            weight_copy(k, 1, sibling).start()
+
+    @pl.when(c == y)
+    def _():
+        for source, target in weights_of:
+            target[c] = source[...]
+
+    def weight_arrived(k):
+        source, target = weights_of[k]
+
+        def wait(h):
+            pltpu.make_async_remote_copy(
+                src_ref=source,
+                dst_ref=target.at[h],
+                send_sem=send_sem.at[2 * k],
+                recv_sem=recv_sem.at[2 * k + h],
+                device_id=sibling,
+                device_id_type=pl.DeviceIdType.MESH,
+            ).wait_recv()
+
+        wait(1 - c)
+
+        @pl.when(c != y)
+        def _():
+            wait(c)
 
     def relay(hop, upward):
         number = (12 if upward else 47) + hop - 1
@@ -263,10 +303,6 @@
                 outgoing().wait_send()
 
     relay_start(1)
-    gate_y[y] = w_gate[...]
-    up_y[y] = w_up[...]
-    down_y[y] = w_down[...]
-
     ids = routing[0:1, :]
     group = lax.shift_right_logical(ids, 1)
     rows16 = lax.broadcasted_iota(jnp.int32, (16, token_count), 0)
@@ -300,6 +336,10 @@
     relay_arrived(1)
     relay_start(2)
 
+    def dispatch(s):
+        send(19 + s, slots_out.at[s], slots.at[s], peer_of[s])
+        send(22 + s, scale_out.at[s], scale.at[s], peer_of[s])
+
     slot_row = lax.broadcasted_iota(jnp.int32, (capacity, token_count), 0)
     for s in (2, 3, 1, 0):
         wanted = (slot_row + level[s] * capacity).astype(F32)
@@ -313,21 +353,13 @@
         else:
             slots_out[s] = rows
             scale_out[s] = slot_weights
-            send(19 + s, slots_out.at[s], slots.at[s], peer_of[s])
-            send(22 + s, scale_out.at[s], scale.at[s], peer_of[s])
-
-    def share(number, stage):
-        arrived(number)
-        whole, rest = stage
-        send(number + 3, whole.at[1 - c], rest, sibling)
-
-    def project(s, start):
+            if s > 1:
+                dispatch(s)
+
+    def project(s, start, weights):
         own = slots[s, pl.ds(start, half), :]
         other = slots_s[s, pl.ds(start, half), :]
-        return (
-            dot(own, gate_y[c]) + dot(other, gate_s[...]),
-            dot(own, up_y[c]) + dot(other, up_s[...]),
-        )
+        return dot(own, weights[c]) + dot(other, weights[1 - c])
 
     mine = pl.multiple_of(x * half, half)
     theirs = pl.multiple_of((1 - x) * half, half)
@@ -337,18 +369,26 @@
             arrived(19 + s)
             send(26 + s, slots.at[s], slots_s.at[s], sibling)
 
+    sides = (slice(0, ff), slice(ff, 2 * ff))
+
     def stage_a(s):
         arrived(26 + s)
-        gate_part, up_part = project(s, theirs)
-        part_out[s, :, :ff] = gate_part.astype(BF16)
-        part_out[s, :, ff:] = up_part.astype(BF16)
+        for side, weights in zip(sides, (gate_all, up_all)):
+            part_out[s, :, side] = project(s, theirs, weights).astype(BF16)
         send(30 + s, part_out.at[s], part_in.at[s], across)
-        gate_part, up_part = project(s, mine)
-        part_own[s, :, :ff] = gate_part
-        part_own[s, :, ff:] = up_part
+        for side, weights in zip(sides, (gate_all, up_all)):
+            part_own[s, :, side] = project(s, mine, weights)
+
+    def stage_a_own(k):
+        side, weights = sides[k], (gate_all, up_all)[k]
+        part_out[0, :, side] = project(0, theirs, weights).astype(BF16)
+        send(30 + 20 * k, part_out.at[0, :, side], part_in.at[0, :, side], across)
+        part_own[0, :, side] = project(0, mine, weights)
 
     def stage_b(s):
         arrived(30 + s)
+        if s == 0:
+            arrived(50)
         gate_sum = part_own[s, :, :ff] + part_in[s, :, :ff].astype(F32)
         up_sum = part_own[s, :, ff:] + part_in[s, :, ff:].astype(F32)
         hidden[s, pl.ds(mine, half), :] = (silu(gate_sum) * up_sum).astype(BF16)
@@ -362,9 +402,9 @@
         columns = jnp.transpose(scale[s])
         weight = jnp.where(c == 0, columns[:, 0:1], columns[:, 1:2])
         units = hidden[s]
-        half_out[s] = (dot(units, down_s[...]) * weight).astype(BF16)
+        half_out[s] = (dot(units, down_all[1 - c]) * weight).astype(BF16)
         send(38 + s, half_out.at[s], half_in.at[s], sibling)
-        half_own[s] = dot(units, down_y[c]) * weight
+        half_own[s] = dot(units, down_all[c]) * weight
 
     def stage_d(s):
         arrived(38 + s)
@@ -375,32 +415,32 @@
             back_out[s] = both
             send(41 + s, back_out.at[s], back.at[s], peer_of[s])
 
-    share(0, (gate_y, gate_s))
+    weight_arrived(0)
+    arrived(26)
+    stage_a_own(0)
+    dispatch(1)
     relay_arrived(2)
     relay_start(3)
+    weight_arrived(1)
+    stage_a_own(1)
     forward(2)
-    share(1, (up_y, up_s))
-    arrived(3)
-    arrived(4)
-    stage_a(2)
-    stage_a(0)
     arrived(10)
     send(11, normed.at[2], normed.at[3], sibling)
-    share(2, (down_y, down_s))
+    stage_a(2)
     relay_arrived(3)
     send(18, branch_all.at[y], branch_all.at[y], pair)
-    stage_b(2)
+    stage_b(0)
     forward(3)
     stage_a(3)
-    stage_b(0)
-    arrived(5)
-    stage_c(2)
-    stage_d(2)
+    stage_b(2)
+    weight_arrived(2)
+    stage_c(0)
+    stage_d(0)
     forward(1)
     stage_a(1)
     stage_b(3)
-    stage_c(0)
-    stage_d(0)
+    stage_c(2)
+    stage_d(2)
 
     arrived(9)
     arrived(11)
@@ -457,6 +497,13 @@
         copy.wait_send()
     for hop in range(1, GROUPS):
         relay_sent(hop)
+    for k in range(3):
+        weight_copy(k, 0, pair_user).wait_send()
+
+    @pl.when(c != y)
+    def _():
+        for k in range(3):
+            weight_copy(k, 1, sibling).wait_send()
 
 
 def pair_body(
@@ -482,9 +529,6 @@
         vmem((2, quarter, ff), BF16),
         vmem((2, quarter, ff), BF16),
         vmem((2, ff, quarter), BF16),
-        vmem((quarter, ff), BF16),
-        vmem((quarter, ff), BF16),
-        vmem((ff, quarter), BF16),
         vmem((4, 8, count), F32),
         vmem((4, count, quarter), BF16),
         vmem((2, GROUPS, 2, block, block), BF16),

time: 124 us -> 115 us (0.927)
  Pallas kernels: 122 us -> 113 us
    pallas_call x1, Pallas kernels: 122 us -> 113 us  [pair_body(): pl.pallas_call(pair_kernel, out_shape=jax.ShapeDtypeStruct((count, quarte...]
where the time goes in v3:
time: 115 us
  Pallas kernels  113 us (98%)
  local copies, waits for them, and re-layouts  2.06 us (2%)
    pallas_call x1, Pallas kernels, pair_body(): pl.pallas_call(pair_kernel, out_shape=jax.ShapeDtypeStruct((count, quarte...  113 us

profile of v3, /device:TPU:0, one launch (start us, length us, event | category | flops | bytes accessed | tf_op | source)
XLA Modules:
  0.0 115.1 jit_solution(16331947350779618908)
XLA Ops:
  0.0 113.0 %shard_map.100 = bf16[768,512]{1,0:T(8,128)(2,1)} custom-call(bf16[768,512]{1,0:T(8,128)(2,1)} %tokens.1, f32[1,512]{1,0:T(1,128)} %bitcast.12, s32[2,768]{1,0:T(2,128)} %bitcast.10, f32[2,768]{1,0:T(2,128)} %bitcast.11, bf16[512,512]{1,0:T(8,128)(2,1)} %bitcast.7, bf16[512,512]{1,0:T(8,128)(2,1)} %bitcast.8, bf16[512,512]{1,0:T(8,128)(2,1)} %bitcast.9, ...), custom_call_target="tpu_custom_call" | custom-call | tf_op jit(solution)/shard_map/pallas_call | solution.py:559
  113.0 2.1 %copy.12 = bf16[768,512]{1,0:T(8,128)(2,1)} copy(bf16[768,512]{1,0:T(8,128)(2,1)} %shard_map.100) | data formatting | bytes 1572864

commit v4 on v3

--- a/solution.py
+++ b/solution.py
@@ -333,8 +333,6 @@
     normed[0] = (tokens[...].astype(F32) * factor_col * gain[...]).astype(BF16)
     send(10, normed.at[0], normed.at[2], across)
     send(9, normed.at[0], normed.at[1], sibling)
-    relay_arrived(1)
-    relay_start(2)
 
     def dispatch(s):
         send(19 + s, slots_out.at[s], slots.at[s], peer_of[s])
@@ -418,29 +416,33 @@
     weight_arrived(0)
     arrived(26)
     stage_a_own(0)
+    weight_arrived(1)
+    stage_a_own(1)
     dispatch(1)
+    relay_arrived(1)
+    relay_start(2)
+    forward(2)
+    stage_a(2)
+    arrived(10)
+    send(11, normed.at[2], normed.at[3], sibling)
     relay_arrived(2)
     relay_start(3)
-    weight_arrived(1)
-    stage_a_own(1)
-    forward(2)
-    arrived(10)
-    send(11, normed.at[2], normed.at[3], sibling)
-    stage_a(2)
-    relay_arrived(3)
-    send(18, branch_all.at[y], branch_all.at[y], pair)
-    stage_b(0)
     forward(3)
     stage_a(3)
     stage_b(2)
+    relay_arrived(3)
+    send(18, branch_all.at[y], branch_all.at[y], pair)
+    stage_b(3)
+    stage_b(0)
     weight_arrived(2)
-    stage_c(0)
-    stage_d(0)
+    stage_c(2)
     forward(1)
     stage_a(1)
-    stage_b(3)
-    stage_c(2)
     stage_d(2)
+    stage_c(3)
+    stage_c(0)
+    stage_d(3)
+    stage_d(0)
 
     arrived(9)
     arrived(11)
@@ -462,8 +464,6 @@
     send(45, fold_out, fold_in, sibling)
 
     stage_b(1)
-    stage_c(3)
-    stage_d(3)
 
     arrived(45)
     for side in range(2):

time: 115 us -> 113 us (0.983); the launches traced: 115 us -> 111 us
  Pallas kernels: 113 us -> 109 us
    pallas_call x1, Pallas kernels: 113 us -> 109 us  [pair_body(): pl.pallas_call(pair_kernel, out_shape=jax.ShapeDtypeStruct((count, quarte...]
where the time goes in v4:
time: 113 us; the launch traced here: 111 us
  Pallas kernels  109 us (96%)
  local copies, waits for them, and re-layouts  2.06 us (2%)
    pallas_call x1, Pallas kernels, pair_body(): pl.pallas_call(pair_kernel, out_shape=jax.ShapeDtypeStruct((count, quarte...  109 us

profile of v4, /device:TPU:0, one launch (start us, length us, event | category | flops | bytes accessed | tf_op | source)
XLA Modules:
  0.0 111.5 jit_solution(3482500550220921952)
XLA Ops:
  0.0 109.4 %shard_map.100 = bf16[768,512]{1,0:T(8,128)(2,1)} custom-call(bf16[768,512]{1,0:T(8,128)(2,1)} %tokens.1, f32[1,512]{1,0:T(1,128)} %bitcast.12, s32[2,768]{1,0:T(2,128)} %bitcast.10, f32[2,768]{1,0:T(2,128)} %bitcast.11, bf16[512,512]{1,0:T(8,128)(2,1)} %bitcast.7, bf16[512,512]{1,0:T(8,128)(2,1)} %bitcast.8, bf16[512,512]{1,0:T(8,128)(2,1)} %bitcast.9, ...), custom_call_target="tpu_custom_call" | custom-call | tf_op jit(solution)/shard_map/pallas_call | solution.py:559
  109.4 2.1 %copy.12 = bf16[768,512]{1,0:T(8,128)(2,1)} copy(bf16[768,512]{1,0:T(8,128)(2,1)} %shard_map.100) | data formatting | bytes 1572864

commit v5 on v4

--- a/solution.py
+++ b/solution.py
@@ -413,6 +413,10 @@
             back_out[s] = both
             send(41 + s, back_out.at[s], back.at[s], peer_of[s])
 
+    def pair_send(m):
+        rows = branch_all.at[y, level[m]]
+        send(15 + m, rows, rows, pair)
+
     weight_arrived(0)
     arrived(26)
     stage_a_own(0)
@@ -421,19 +425,22 @@
     dispatch(1)
     relay_arrived(1)
     relay_start(2)
+    pair_send(0)
+    pair_send(1)
     forward(2)
     stage_a(2)
     arrived(10)
     send(11, normed.at[2], normed.at[3], sibling)
+    forward(3)
+    stage_a(3)
     relay_arrived(2)
     relay_start(3)
-    forward(3)
-    stage_a(3)
+    pair_send(2)
     stage_b(2)
-    relay_arrived(3)
-    send(18, branch_all.at[y], branch_all.at[y], pair)
     stage_b(3)
     stage_b(0)
+    relay_arrived(3)
+    pair_send(3)
     weight_arrived(2)
     stage_c(2)
     forward(1)
@@ -446,7 +453,8 @@
 
     arrived(9)
     arrived(11)
-    arrived(18)
+    for m in range(GROUPS):
+        arrived(15 + m)
     quarters = (tp, x * 2 + 1 - c, (1 - x) * 2 + c, (1 - x) * 2 + 1 - c)
     sums = jnp.zeros((token_count, block), F32)
     for k, q in enumerate(quarters):

time: 113 us -> 110 us (0.973)
  Pallas kernels: 109 us -> 107 us
    pallas_call x1, Pallas kernels: 109 us -> 107 us  [pair_body(): pl.pallas_call(pair_kernel, out_shape=jax.ShapeDtypeStruct((count, quarte...]
where the time goes in v5:
time: 110 us; the launch traced here: 109 us
  Pallas kernels  107 us (97%)
  local copies, waits for them, and re-layouts  2.06 us (2%)
    pallas_call x1, Pallas kernels, pair_body(): pl.pallas_call(pair_kernel, out_shape=jax.ShapeDtypeStruct((count, quarte...  107 us

profile of v5, /device:TPU:0, one launch (start us, length us, event | category | flops | bytes accessed | tf_op | source)
XLA Modules:
  0.0 109.5 jit_solution(11383371066893136359)
XLA Ops:
  0.0 107.4 %shard_map.100 = bf16[768,512]{1,0:T(8,128)(2,1)} custom-call(bf16[768,512]{1,0:T(8,128)(2,1)} %tokens.1, f32[1,512]{1,0:T(1,128)} %bitcast.12, s32[2,768]{1,0:T(2,128)} %bitcast.10, f32[2,768]{1,0:T(2,128)} %bitcast.11, bf16[512,512]{1,0:T(8,128)(2,1)} %bitcast.7, bf16[512,512]{1,0:T(8,128)(2,1)} %bitcast.8, bf16[512,512]{1,0:T(8,128)(2,1)} %bitcast.9, ...), custom_call_target="tpu_custom_call" | custom-call | tf_op jit(solution)/shard_map/pallas_call | solution.py:567
  107.4 2.1 %copy.12 = bf16[768,512]{1,0:T(8,128)(2,1)} copy(bf16[768,512]{1,0:T(8,128)(2,1)} %shard_map.100) | data formatting | bytes 1572864

commit v6 on v5

--- a/solution.py
+++ b/solution.py
@@ -431,6 +431,7 @@
     stage_a(2)
     arrived(10)
     send(11, normed.at[2], normed.at[3], sibling)
+    stage_b(0)
     forward(3)
     stage_a(3)
     relay_arrived(2)
@@ -438,7 +439,6 @@
     pair_send(2)
     stage_b(2)
     stage_b(3)
-    stage_b(0)
     relay_arrived(3)
     pair_send(3)
     weight_arrived(2)

time: 110 us -> 110 us (level)
  no operation moved by 1% of the time
where the time goes in v6:
time: 110 us; the launch traced here: 109 us
  Pallas kernels  107 us (97%)
  local copies, waits for them, and re-layouts  2.06 us (2%)
    pallas_call x1, Pallas kernels, pair_body(): pl.pallas_call(pair_kernel, out_shape=jax.ShapeDtypeStruct((count, quarte...  107 us

profile of v6, /device:TPU:0, one launch (start us, length us, event | category | flops | bytes accessed | tf_op | source)
XLA Modules:
  0.0 109.4 jit_solution(3779288972032764048)
XLA Ops:
  0.0 107.3 %shard_map.100 = bf16[768,512]{1,0:T(8,128)(2,1)} custom-call(bf16[768,512]{1,0:T(8,128)(2,1)} %tokens.1, f32[1,512]{1,0:T(1,128)} %bitcast.12, s32[2,768]{1,0:T(2,128)} %bitcast.10, f32[2,768]{1,0:T(2,128)} %bitcast.11, bf16[512,512]{1,0:T(8,128)(2,1)} %bitcast.7, bf16[512,512]{1,0:T(8,128)(2,1)} %bitcast.8, bf16[512,512]{1,0:T(8,128)(2,1)} %bitcast.9, ...), custom_call_target="tpu_custom_call" | custom-call | tf_op jit(solution)/shard_map/pallas_call | solution.py:567
  107.3 2.1 %copy.12 = bf16[768,512]{1,0:T(8,128)(2,1)} copy(bf16[768,512]{1,0:T(8,128)(2,1)} %shard_map.100) | data formatting | bytes 1572864
